TPU v7x, 32 devices: a whole 2x2x4 slice. The times are simulated.
32 devices in a mesh: grp: 2 (over y), fs: 4 (over z), tp: 4 (over x, core).
Axes of the slice: x: 2, y: 2, z: 4, core: 2. Of those that a mesh axis runs over, the one named last changes fastest.
Arguments:
- tokens: bfloat16 [2560, 2048], P(('grp', 'fs', 'tp')), parts along dimension 0, may hold values from -6 to 6
- mix_gain: bfloat16 [2048], replicated, may hold values from 0.099609375 to 1.8984375
- val_weight: bfloat16 [2048, 1024], P('fs', 'tp'), may hold values from -4 to 4
- gate_weight: bfloat16 [2048, 1024], P('fs', 'tp'), may hold values from -0.125 to 0.125
- conv_taps: bfloat16 [31, 1024], replicated, may hold values from -1 to 1
- chan_gain: bfloat16 [1024], replicated, may hold values from 0.099609375 to 1.8984375
- out_weight: bfloat16 [1024, 2048], P('tp', 'fs'), may hold values from -0.1875 to 0.1875
- mix_post_gain: bfloat16 [2048], replicated, may hold values from 0.099609375 to 1.8984375
- ffn_gain: bfloat16 [2048], replicated, may hold values from 0.099609375 to 1.8984375
- up_gate_weight: bfloat16 [2048, 5120], P('fs', 'tp'), may hold values from -0.125 to 0.125
- up_val_weight: bfloat16 [2048, 5120], P('fs', 'tp'), may hold values from -0.125 to 0.125
- ffn_taps: bfloat16 [2, 3, 5120], replicated, may hold values from -3.5 to 3.5
- down_weight: bfloat16 [5120, 2048], P('tp', 'fs'), may hold values from -0.078125 to 0.078125
- ffn_post_gain: bfloat16 [2048], replicated, may hold values from 0.099609375 to 1.8984375
Outputs:
- layer_out: bfloat16 [2560, 2048], P(('grp', 'fs', 'tp')), parts along dimension 0
There are 2 independent parts, one for each index of `grp`. A program takes and returns all parts, laid end to end along the dimension named above; an argument that names none is the same for every part. Nothing has to cross between parts.
All inputs are finite; a program needn't handle non-finite values.
Results may differ from a plain program's by a relative error of at most 0.019.
Values may be sent and summed in bfloat16 or wider, within the bound.
A program may use at most 64 MiB of HBM per device.

v0:
```python
import jax
import jax.numpy as jnp
from jax import lax
from jax.sharding import PartitionSpec as P

LEN = 64


norm_epsilon = 1e-06
chan_epsilon = 1e-05


def rms_scale(values, gain):
    inverse = lax.rsqrt(jnp.mean(values * values, axis=-1, keepdims=True) + norm_epsilon)
    return values * inverse * gain.astype(jnp.float32)


def depthwise(signal, tap_table):
    taps_count = tap_table.shape[0]
    channels = signal.shape[1]
    shaped = signal.astype(jnp.float32).reshape(signal.shape[0] // LEN, LEN, channels)
    padded = jnp.pad(shaped, ((0, 0), (taps_count - 1, 0), (0, 0)))
    tap_values = tap_table.astype(jnp.float32)
    result = jnp.zeros(shaped.shape, jnp.float32)
    for offset in range(taps_count):
        result = result + padded[:, offset : offset + LEN, :] * tap_values[offset]
    return result.reshape(signal.shape[0], channels)


def make_adder(left, pieces):
    first = jnp.dot(left, pieces[0], preferred_element_type=jnp.float32)
    second = jnp.dot(left, pieces[1], preferred_element_type=jnp.float32)
    return (first, second)


def make_rows_product(left, weight):
    return jnp.dot(left, weight, preferred_element_type=jnp.float32)


def shards(
    tokens,
    mix_gain,
    val_weight,
    gate_weight,
    conv_taps,
    chan_gain,
    out_weight,
    mix_post_gain,
    ffn_gain,
    up_gate_weight,
    up_val_weight,
    ffn_taps,
    down_weight,
    ffn_post_gain,
):
    member = lax.axis_index("tp")
    normed_own = rms_scale(tokens.astype(jnp.float32), mix_gain).astype(jnp.bfloat16)
    normed = lax.all_gather(normed_own, "tp", axis=0, tiled=True)
    local_ch = val_weight.shape[1]
    values, gate_sums = make_adder(
        normed,
        (
            lax.all_gather(val_weight, "fs", axis=0, tiled=True),
            lax.all_gather(gate_weight, "fs", axis=0, tiled=True),
        ),
    )
    glu_out = (values * jax.nn.sigmoid(gate_sums)).astype(jnp.bfloat16)
    own_taps = lax.dynamic_slice_in_dim(conv_taps, member * local_ch, local_ch, 1)
    conv_out = depthwise(glu_out, own_taps)
    totals, squares = lax.psum(
        (jnp.sum(conv_out, axis=1), jnp.sum(conv_out * conv_out, axis=1)), "tp"
    )
    all_channels = chan_gain.shape[0]
    chan_mean = totals[:, None] / all_channels
    chan_var = squares[:, None] / all_channels - chan_mean * chan_mean
    own_gain = lax.dynamic_slice_in_dim(chan_gain, member * local_ch, local_ch, 0).astype(
        jnp.float32
    )
    activated = jax.nn.silu((conv_out - chan_mean) * lax.rsqrt(chan_var + chan_epsilon) * own_gain)
    activated = activated.astype(jnp.bfloat16)
    out_full = lax.all_gather(out_weight, "fs", axis=1, tiled=True)
    mixed_sum = lax.psum_scatter(
        make_rows_product(activated, out_full).astype(jnp.bfloat16),
        "tp",
        scatter_dimension=0,
        tiled=True,
    ).astype(jnp.float32)
    residual = (tokens.astype(jnp.float32) + rms_scale(mixed_sum, mix_post_gain)).astype(
        jnp.bfloat16
    )
    normed_share = rms_scale(residual.astype(jnp.float32), ffn_gain).astype(jnp.bfloat16)
    normed_ffn = lax.all_gather(normed_share, "tp", axis=0, tiled=True)
    local_ff = up_gate_weight.shape[1]
    own_ffn_taps = lax.dynamic_slice_in_dim(ffn_taps, member * local_ff, local_ff, 2)
    gate_full, val_full = (
        lax.all_gather(up_gate_weight, "fs", axis=0, tiled=True),
        lax.all_gather(up_val_weight, "fs", axis=0, tiled=True),
    )
    up_gate = jnp.dot(normed_ffn, gate_full, preferred_element_type=jnp.float32).astype(
        jnp.bfloat16
    )
    up_val = jnp.dot(normed_ffn, val_full, preferred_element_type=jnp.float32).astype(jnp.bfloat16)
    gate_conv = depthwise(up_gate, own_ffn_taps[0])
    val_conv = depthwise(up_val, own_ffn_taps[1])
    hidden = (jax.nn.gelu(gate_conv, approximate=True) * val_conv).astype(jnp.bfloat16)
    down_full = lax.all_gather(down_weight, "fs", axis=1, tiled=True)
    ffn_sum = lax.psum_scatter(
        make_rows_product(hidden, down_full).astype(jnp.bfloat16),
        "tp",
        scatter_dimension=0,
        tiled=True,
    ).astype(jnp.float32)
    return (residual.astype(jnp.float32) + rms_scale(ffn_sum, ffn_post_gain)).astype(jnp.bfloat16)


def solution(mesh):
    return jax.shard_map(
        shards,
        mesh=mesh,
        in_specs=(
            P(("grp", "fs", "tp"), None),
            P(),
            P("fs", "tp"),
            P("fs", "tp"),
            P(),
            P(),
            P("tp", "fs"),
            P(),
            P(),
            P("fs", "tp"),
            P("fs", "tp"),
            P(),
            P("tp", "fs"),
            P(),
        ),
        out_specs=P(("grp", "fs", "tp"), None),
        check_vma=False,
    )
```

profile of v0, /device:TPU:0, one launch (start us, length us, event | category | flops | bytes accessed | tf_op | source)
XLA Modules:
  0.0 503.6 jit_solution(17224619364062690328)
XLA Ops:
  6.5 0.7 all-gather.11.cloned.1.call-update
  7.3 0.0 all-gather.9.cloned.1.call-start
  7.3 0.7 convert_element_type.82
  8.0 1.1 fusion.26
  9.1 1.8 fusion.28
  11.0 0.0 all-gather.13.cloned.1.call-start
  11.1 0.7 all-gather.13.cloned.1.call-update
  11.8 0.5 all-gather.15.cloned.1.call-update
  12.3 0.0 reduce-scatter.3.cloned.1.call-start
  12.4 0.7 dynamic-slice_convert_fusion
  13.1 0.8 dynamic-slice_convert_fusion.3
  13.9 25.7 %all-gather.11.cloned.1.call-done = bf16[2048,256]{1,0:T(8,128)(2,1)} async-done(((bf16[512,256]{1,0:T(8,128)(2,1)}), bf16[2048,256]{1,0:T(8,128)(2,1)}) %all-gather.11.cloned.1.call-update) | async-done | bytes 1048592 | tf_op jit(solution)/shard_map/all_gather | solution.py:63
  39.7 19.1 %all-gather.9.cloned.1.call-done = bf16[320,2048]{1,0:T(8,128)(2,1)} async-done(((bf16[80,2048]{1,0:T(8,128)(2,1)}), bf16[320,2048]{1,0:T(8,128)(2,1)}) %all-gather.9.cloned.1.call-update) | async-done | bytes 1310736 | tf_op jit(solution)/shard_map/all_gather | solution.py:58
  58.8 2.2 fusion.101
  61.0 27.4 %all-gather.13.cloned.1.call-done = bf16[2048,256]{1,0:T(8,128)(2,1)} async-done(((bf16[512,256]{1,0:T(8,128)(2,1)}), bf16[2048,256]{1,0:T(8,128)(2,1)}) %all-gather.13.cloned.1.call-update) | async-done | bytes 1048592 | tf_op jit(solution)/shard_map/all_gather | solution.py:64
  88.4 1.7 fusion.21
  90.2 1.2 fusion.96
  91.4 0.1 reduce_sum.60
  91.5 0.1 reduce_sum.62
  91.5 6.1 %all-reduce.3 = (f32[320]{0:T(512)S(1)}, f32[320]{0:T(512)S(1)}) all-reduce(f32[320]{0:T(512)S(1)} %reduce_sum.62, f32[320]{0:T(512)S(1)} %reduce_sum.60), channel_id=1, replica_groups=mesh['grp'=2,'fs'=4,'tp'=4] {'tp'}, use_global_device_ids=true, to_apply=%region_4.5 | all-reduce | flops 640 | bytes 5120 | tf_op jit(solution)/shard_map/psum | solution.py:70
  97.6 0.2 multiply_convert_fusion
  97.8 19.4 %all-gather.15.cloned.1.call-done = bf16[256,2048]{1,0:T(8,128)(2,1)} async-done(((bf16[256,512]{1,0:T(8,128)(2,1)}), bf16[256,2048]{1,0:T(8,128)(2,1)}) %all-gather.15.cloned.1.call-update) | async-done | bytes 1048592 | tf_op jit(solution)/shard_map/all_gather | solution.py:81
  117.2 2.8 convolution_convert_fusion.3
  120.0 0.0 all-gather.17.cloned.1.call-start
  120.1 25.9 %reduce-scatter.3.cloned.1.call-done = bf16[80,2048]{1,0:T(8,128)(2,1)} async-done(((bf16[320,2048]{1,0:T(8,128)(2,1)}), bf16[80,2048]{1,0:T(8,128)(2,1)}) %reduce-scatter.3.cloned.1.call-update) | async-done | bytes 327696 | tf_op jit(solution)/shard_map/reduce_scatter | solution.py:82
  146.0 1.1 fusion.22
  147.1 1.3 fusion.30
  148.5 0.9 fusion.32
  149.4 0.0 all-gather.19.cloned.1.call-start
  149.4 0.7 all-gather.19.cloned.1.call-update
  150.2 0.7 all-gather.21.cloned.1.call-update
  150.9 0.7 all-gather.23.cloned.1.call-update
  151.6 0.0 reduce-scatter.5.cloned.1.call-start
  151.7 0.1 dynamic-slice_convert_fusion.2
  151.9 15.8 %all-gather.17.cloned.1.call-done = bf16[320,2048]{1,0:T(8,128)(2,1)} async-done(((bf16[80,2048]{1,0:T(8,128)(2,1)}), bf16[320,2048]{1,0:T(8,128)(2,1)}) %all-gather.17.cloned.1.call-update) | async-done | bytes 1310736 | tf_op jit(solution)/shard_map/all_gather | solution.py:92
  167.7 99.6 %all-gather.19.cloned.1.call-done = bf16[2048,1280]{1,0:T(8,128)(2,1)} async-done(((bf16[512,1280]{1,0:T(8,128)(2,1)}), bf16[2048,1280]{1,0:T(8,128)(2,1)}) %all-gather.19.cloned.1.call-update) | async-done | bytes 5242896 | tf_op jit(solution)/shard_map/all_gather | solution.py:96
  267.3 4.8 convolution_convert_fusion.2
  272.1 0.1 convert.4
  272.2 93.1 %all-gather.21.cloned.1.call-done = bf16[2048,1280]{1,0:T(8,128)(2,1)} async-done(((bf16[512,1280]{1,0:T(8,128)(2,1)}), bf16[2048,1280]{1,0:T(8,128)(2,1)}) %all-gather.21.cloned.1.call-update) | async-done | bytes 5242896 | tf_op jit(solution)/shard_map/all_gather | solution.py:97
  365.3 4.3 convolution_convert_fusion.1
  369.7 0.1 convert.5
  369.8 1.0 fusion.2
  370.8 0.6 fusion.16
  371.3 92.0 %all-gather.23.cloned.1.call-done = bf16[1280,2048]{1,0:T(8,128)(2,1)} async-done(((bf16[1280,512]{1,0:T(8,128)(2,1)}), bf16[1280,2048]{1,0:T(8,128)(2,1)}) %all-gather.23.cloned.1.call-update) | async-done | bytes 5242896 | tf_op jit(solution)/shard_map/all_gather | solution.py:106
  463.3 5.5 %convolution_convert_fusion = bf16[320,2048]{1,0:T(8,128)(2,1)} fusion(bf16[320,1280]{1,0:T(8,128)(2,1)S(1)} %fusion.16, bf16[1280,2048]{1,0:T(8,128)(2,1)} %all-gather.23.cloned.1.call-done), kind=kOutput, calls=%fused_computation | convolution fusion | flops 1678376960 | bytes 7372800 | tf_op jit(solution)/shard_map/dot_general | solution.py:37
  468.8 24.9 %reduce-scatter.5.cloned.1.call-done = bf16[80,2048]{1,0:T(8,128)(2,1)} async-done(((bf16[320,2048]{1,0:T(8,128)(2,1)}), bf16[80,2048]{1,0:T(8,128)(2,1)}) %reduce-scatter.5.cloned.1.call-update) | async-done | bytes 327696 | tf_op jit(solution)/shard_map/reduce_scatter | solution.py:107
  493.7 1.1 fusion.24
  494.9 1.9 fusion.33
  (35 shorter events, 0.4 us)
Async XLA Ops:
  6.5 33.1 %all-gather.11.cloned.1.call-start = ((), (), s32[]{:S(2)}) async-start(), calls=%async_computation.3 | async-start | bytes 1310720 | tf_op jit(solution)/shard_map/all_gather | solution.py:63
  7.3 51.5 %all-gather.9.cloned.1.call-start = ((), (), s32[]{:S(2)}) async-start(), calls=%async_computation.2 | async-start | bytes 1638400 | tf_op jit(solution)/shard_map/all_gather | solution.py:58
  11.0 77.4 %all-gather.13.cloned.1.call-start = ((), (), s32[]{:S(2)}) async-start(), calls=%async_computation.4 | async-start | bytes 1310720 | tf_op jit(solution)/shard_map/all_gather | solution.py:64
  11.8 105.4 %all-gather.15.cloned.1.call-start = ((), (), s32[]{:S(2)}) async-start(), calls=%async_computation.5 | async-start | bytes 1310720 | tf_op jit(solution)/shard_map/all_gather | solution.py:81
  12.3 133.6 %reduce-scatter.3.cloned.1.call-start = ((), (), s32[]{:S(2)}) async-start(), calls=%async_computation.6 | async-start | bytes 1638400 | tf_op jit(solution)/shard_map/reduce_scatter | solution.py:82
  58.8 29.6 %copy-start.5 = (bf16[320,2048]{1,0:T(8,128)(2,1)S(1)}, bf16[320,2048]{1,0:T(8,128)(2,1)}, u32[]{:S(2)}) copy-start(bf16[320,2048]{1,0:T(8,128)(2,1)} %all-gather.9.cloned.1.call-done) | copy-start | bytes 3932164
  97.8 22.3 %copy-start.2 = (bf16[2048]{0:T(1024)(128)(2,1)S(1)}, bf16[2048]{0:T(1024)(128)(2,1)}, u32[]{:S(2)}) copy-start(bf16[2048]{0:T(1024)(128)(2,1)} %param.21) | copy-start | bytes 12292
  97.8 22.3 %copy-start.3 = (bf16[2048]{0:T(1024)(128)(2,1)S(1)}, bf16[2048]{0:T(1024)(128)(2,1)}, u32[]{:S(2)}) copy-start(bf16[2048]{0:T(1024)(128)(2,1)} %param.22) | copy-start | bytes 12292
  97.8 49.3 %copy-start = (bf16[80,2048]{1,0:T(8,128)(2,1)S(1)}, bf16[80,2048]{1,0:T(8,128)(2,1)}, u32[]{:S(2)}) copy-start(bf16[80,2048]{1,0:T(8,128)(2,1)} %param.14) | copy-start | bytes 983044
  120.0 47.7 %all-gather.17.cloned.1.call-start = ((), (), s32[]{:S(2)}) async-start(), calls=%async_computation.7 | async-start | bytes 1638400 | tf_op jit(solution)/shard_map/all_gather | solution.py:92
  149.4 118.0 %all-gather.19.cloned.1.call-start = ((), (), s32[]{:S(2)}) async-start(), calls=%async_computation.8 | async-start | bytes 6553600 | tf_op jit(solution)/shard_map/all_gather | solution.py:96
  150.1 1.5 copy-start.1
  150.1 215.2 %all-gather.21.cloned.1.call-start = ((), (), s32[]{:S(2)}) async-start(), calls=%async_computation.9 | async-start | bytes 6553600 | tf_op jit(solution)/shard_map/all_gather | solution.py:97
  150.9 312.4 %all-gather.23.cloned.1.call-start = ((), (), s32[]{:S(2)}) async-start(), calls=%async_computation.10 | async-start | bytes 6553600 | tf_op jit(solution)/shard_map/all_gather | solution.py:106
  151.6 342.1 %reduce-scatter.5.cloned.1.call-start = ((), (), s32[]{:S(2)}) async-start(), calls=%async_computation.11 | async-start | bytes 1638400 | tf_op jit(solution)/shard_map/reduce_scatter | solution.py:107
  272.1 93.2 %copy-start.6 = (bf16[320,2048]{1,0:T(8,128)(2,1)S(1)}, bf16[320,2048]{1,0:T(8,128)(2,1)}, u32[]{:S(2)}) copy-start(bf16[320,2048]{1,0:T(8,128)(2,1)} %all-gather.17.cloned.1.call-done) | copy-start | bytes 3932164
  371.3 97.5 %copy-start.4 = (bf16[2048]{0:T(1024)(128)(2,1)S(1)}, bf16[2048]{0:T(1024)(128)(2,1)}, u32[]{:S(2)}) copy-start(bf16[2048]{0:T(1024)(128)(2,1)} %param.27) | copy-start | bytes 12292
Sparse Core Ops, SparseCore 0:
  8.9 30.7 all-gather.10
  41.2 17.5 all-gather.8
  60.4 27.9 all-gather.12
  89.8 27.3 all-gather.14
  120.1 25.7 reduce-scatter.2
  149.5 18.1 all-gather.16
  169.3 98.0 all-gather.18
  268.9 96.3 all-gather.20
  366.9 96.3 all-gather.22
  468.9 24.7 reduce-scatter.4
where the time goes:
time: 504 us
  waiting for transfers between devices  447 us (89%)
  matrix products  21.4 us (4%)
  other arithmetic  14.9 us (3%)
  between operations  13.8 us (3%)
  blocking collectives  6.05 us (1%)
    all_gather x1, waiting for transfers between devices, shards(): lax.all_gather(up_gate_weight, 'fs', axis=0, tiled=True)  99.6 us
    all_gather x1, waiting for transfers between devices, shards(): lax.all_gather(up_val_weight, 'fs', axis=0, tiled=True)  93.1 us
    all_gather x1, waiting for transfers between devices, shards(): down_full = lax.all_gather(down_weight, 'fs', axis=1, tiled=True)  92 us
    all_gather x1, waiting for transfers between devices, shards(): lax.all_gather(gate_weight, 'fs', axis=0, tiled=True)  27.4 us
    reduce_scatter x1, waiting for transfers between devices, shards(): lax.psum_scatter(make_rows_product(activated, out_full).astype(jnp.bfloat...  25.9 us
    all_gather x1, waiting for transfers between devices, shards(): lax.all_gather(val_weight, 'fs', axis=0, tiled=True)  25.7 us
    reduce_scatter x1, waiting for transfers between devices, shards(): lax.psum_scatter(make_rows_product(hidden, down_full).astype(jnp.bfloat16...  24.9 us
    all_gather x1, waiting for transfers between devices, shards(): out_full = lax.all_gather(out_weight, 'fs', axis=1, tiled=True)  19.4 us
  transfers between devices with their start and end apart: 10, of which 10 were waited for; matrix products, arithmetic and copies ran while one was open for 4% of the time, Pallas kernels for 0%

commit v1 on v0

--- a/solution.py
+++ b/solution.py
@@ -1,6 +1,10 @@
+import functools
+
 import jax
 import jax.numpy as jnp
 from jax import lax
+from jax.experimental import pallas as pl
+from jax.experimental.pallas import tpu as pltpu
 from jax.sharding import PartitionSpec as P
 
 LEN = 64
@@ -37,7 +41,182 @@
     return jnp.dot(left, weight, preferred_element_type=jnp.float32)
 
 
+class LineGather:
+    def __init__(self, count, sources, gathered, semaphores):
+        self.count = count
+        self.sources = sources
+        self.gathered = gathered
+        self.z_send, self.z_recv, self.y_send, self.y_recv, self.own_sem = semaphores
+        self.place = lax.axis_index("fs")
+        self.half = lax.axis_index("grp")
+
+    def barrier(self, extra=()):
+        place, count = self.place, self.count
+        semaphore = pltpu.get_barrier_semaphore()
+        for step in (1, -1):
+
+            @pl.when(self.has(step, 1))
+            def _():
+                pl.semaphore_signal(semaphore, inc=1, device_id={"fs": place + step})
+
+        others = [{"grp": 1 - self.half}] + list(extra)
+        for other in others:
+            pl.semaphore_signal(semaphore, inc=1, device_id=other)
+        inner = (place > 0).astype(jnp.int32) + (place < count - 1).astype(jnp.int32)
+        pl.semaphore_wait(semaphore, inner + len(others))
+
+    def has(self, step, distance):
+        if step > 0:
+            return self.place + distance < self.count
+        return self.place >= distance
+
+    def rows(self, index, half):
+        size = self.sources[index].shape[0] // 2
+        return pl.ds(pl.multiple_of(half * size, size), size)
+
+    def z_copy(self, index, way, distance):
+        step = 1 if way == 0 else -1
+        origin = self.place - step * distance
+        rows = self.rows(index, self.half)
+        target = self.gathered[index].at[origin, rows]
+        source = self.sources[index].at[rows] if distance == 0 else target
+        return pltpu.make_async_remote_copy(
+            src_ref=source,
+            dst_ref=target,
+            send_sem=self.z_send.at[index, way, distance],
+            recv_sem=self.z_recv.at[index, way, distance],
+            device_id={"fs": self.place + step},
+        )
+
+    def z_arrival(self, index, way, distance):
+        step = 1 if way == 0 else -1
+        origin = self.place - step * distance
+        target = self.gathered[index].at[origin, self.rows(index, self.half)]
+        return pltpu.make_async_remote_copy(
+            src_ref=target,
+            dst_ref=target,
+            send_sem=self.z_send.at[index, way, distance - 1],
+            recv_sem=self.z_recv.at[index, way, distance - 1],
+            device_id={"fs": self.place - step},
+        )
+
+    def y_copy(self, index, way, distance, incoming=False):
+        step = 1 if way == 0 else -1
+        origin = self.place - step * distance
+        half = 1 - self.half if incoming else self.half
+        target = self.gathered[index].at[origin, self.rows(index, half)]
+        return pltpu.make_async_remote_copy(
+            src_ref=target,
+            dst_ref=target,
+            send_sem=self.y_send.at[index, way, distance - 1],
+            recv_sem=self.y_recv.at[index, way, distance - 1],
+            device_id={"grp": 1 - self.half},
+        )
+
+    def own_copy(self, index):
+        return pltpu.make_async_copy(
+            self.sources[index], self.gathered[index].at[self.place], self.own_sem.at[index]
+        )
+
+    def start(self, index):
+        for way in range(2):
+
+            @pl.when(self.has(1 - 2 * way, 1))
+            def _():
+                self.z_copy(index, way, 0).start()
+
+        self.own_copy(index).start()
+
+    def relay(self, index, distance):
+        for way in range(2):
+            step = 1 - 2 * way
+
+            @pl.when(self.has(-step, distance))
+            def _():
+                self.z_arrival(index, way, distance).wait_recv()
+                if distance < self.count - 1:
+
+                    @pl.when(self.has(step, 1))
+                    def _():
+                        self.z_copy(index, way, distance).start()
+
+                self.y_copy(index, way, distance).start()
+
+    def arrive(self, index):
+        self.own_copy(index).wait()
+        for distance in range(1, self.count):
+            for way in range(2):
+
+                @pl.when(self.has(2 * way - 1, distance))
+                def _():
+                    self.y_copy(index, way, distance, incoming=True).wait_recv()
+
+    def drain(self, index):
+        for distance in range(self.count):
+            for way in range(2):
+                step = 1 - 2 * way
+                if distance < self.count - 1:
+
+                    @pl.when(jnp.logical_and(self.has(-step, distance), self.has(step, 1)))
+                    def _():
+                        self.z_copy(index, way, distance).wait_send()
+
+                if distance > 0:
+
+                    @pl.when(self.has(-step, distance))
+                    def _():
+                        self.y_copy(index, way, distance).wait_send()
+
+
+def gather_semaphores(weights, count):
+    hops = pltpu.SemaphoreType.DMA((weights, 2, count - 1))
+    return [hops, hops, hops, hops, pltpu.SemaphoreType.DMA((weights,))]
+
+
+def gather_kernel(count, weights, *refs):
+    gather = LineGather(count, refs[:weights], refs[weights : 2 * weights], refs[2 * weights :])
+    gather.barrier()
+    gather.start(0)
+    for index in range(weights):
+        if index + 1 < weights:
+            gather.start(index + 1)
+        for distance in range(1, count):
+            gather.relay(index, distance)
+    for index in range(weights):
+        gather.arrive(index)
+    for index in range(weights):
+        gather.drain(index)
+
+
+def gather_all(count, weights):
+    return pl.pallas_call(
+        functools.partial(gather_kernel, count, len(weights)),
+        out_shape=[jax.ShapeDtypeStruct((count,) + w.shape, w.dtype) for w in weights],
+        in_specs=[pl.BlockSpec(memory_space=pl.ANY)] * len(weights),
+        out_specs=[pl.BlockSpec(memory_space=pltpu.VMEM)] * len(weights),
+        scratch_shapes=gather_semaphores(len(weights), count),
+        compiler_params=pltpu.CompilerParams(
+            collective_id=0, has_side_effects=True, vmem_limit_bytes=60_000_000
+        ),
+    )(*weights)
+
+
+def gather_plain(weights):
+    return [lax.all_gather(w, "fs", axis=0, tiled=False) for w in weights]
+
+
+def fits(mesh, weights):
+    count = mesh.shape["fs"]
+    return (
+        mesh.shape["grp"] == 2
+        and 2 <= count <= 4
+        and all(w.shape[0] % 64 == 0 and w.shape[1] % 128 == 0 for w in weights)
+        and count * sum(w.size for w in weights) <= 20_000_000
+    )
+
+
 def shards(
+    mesh,
     tokens,
     mix_gain,
     val_weight,
@@ -54,14 +233,22 @@
     ffn_post_gain,
 ):
     member = lax.axis_index("tp")
+    weights = (val_weight, gate_weight, out_weight, up_gate_weight, up_val_weight, down_weight)
+    if fits(mesh, weights):
+        pieces = gather_all(mesh.shape["fs"], weights)
+    else:
+        pieces = gather_plain(weights)
+    val_all, gate_all, gate_full, val_full = (
+        pieces[i].reshape(-1, pieces[i].shape[2]) for i in (0, 1, 3, 4)
+    )
     normed_own = rms_scale(tokens.astype(jnp.float32), mix_gain).astype(jnp.bfloat16)
     normed = lax.all_gather(normed_own, "tp", axis=0, tiled=True)
     local_ch = val_weight.shape[1]
     values, gate_sums = make_adder(
         normed,
         (
-            lax.all_gather(val_weight, "fs", axis=0, tiled=True),
-            lax.all_gather(gate_weight, "fs", axis=0, tiled=True),
+            val_all,
+            gate_all,
         ),
     )
     glu_out = (values * jax.nn.sigmoid(gate_sums)).astype(jnp.bfloat16)
@@ -78,7 +265,7 @@
     )
     activated = jax.nn.silu((conv_out - chan_mean) * lax.rsqrt(chan_var + chan_epsilon) * own_gain)
     activated = activated.astype(jnp.bfloat16)
-    out_full = lax.all_gather(out_weight, "fs", axis=1, tiled=True)
+    out_full = jnp.concatenate(list(pieces[2]), axis=1)
     mixed_sum = lax.psum_scatter(
         make_rows_product(activated, out_full).astype(jnp.bfloat16),
         "tp",
@@ -92,10 +279,6 @@
     normed_ffn = lax.all_gather(normed_share, "tp", axis=0, tiled=True)
     local_ff = up_gate_weight.shape[1]
     own_ffn_taps = lax.dynamic_slice_in_dim(ffn_taps, member * local_ff, local_ff, 2)
-    gate_full, val_full = (
-        lax.all_gather(up_gate_weight, "fs", axis=0, tiled=True),
-        lax.all_gather(up_val_weight, "fs", axis=0, tiled=True),
-    )
     up_gate = jnp.dot(normed_ffn, gate_full, preferred_element_type=jnp.float32).astype(
         jnp.bfloat16
     )
@@ -103,7 +286,7 @@
     gate_conv = depthwise(up_gate, own_ffn_taps[0])
     val_conv = depthwise(up_val, own_ffn_taps[1])
     hidden = (jax.nn.gelu(gate_conv, approximate=True) * val_conv).astype(jnp.bfloat16)
-    down_full = lax.all_gather(down_weight, "fs", axis=1, tiled=True)
+    down_full = jnp.concatenate(list(pieces[5]), axis=1)
     ffn_sum = lax.psum_scatter(
         make_rows_product(hidden, down_full).astype(jnp.bfloat16),
         "tp",
@@ -115,7 +298,7 @@
 
 def solution(mesh):
     return jax.shard_map(
-        shards,
+        functools.partial(shards, mesh),
         mesh=mesh,
         in_specs=(
             P(("grp", "fs", "tp"), None),

time: 504 us -> 321 us (0.64)
  waiting for transfers between devices: 447 us -> 65.1 us
  Pallas kernels: 0 us -> 195 us
  local copies, waits for them, and re-layouts: 0.3 us -> 8.17 us
    all_gather x6 -> x0, waiting for transfers between devices: 357 us -> none  [the longest x1 99.6 us: shards(): lax.all_gather(up_gate_weight, 'fs', axis=0, tiled=True)]
    pallas_call x0 -> x1, Pallas kernels: none -> 195 us  [gather_all(): pl.pallas_call(functools.partial(gather_kernel, count, len(weights)), out...]
    all_gather x1, waiting for transfers between devices: 19.1 us -> 0.02 us  [shards(): normed = lax.all_gather(normed_own, 'tp', axis=0, tiled=True)]
    another operation x0 -> x2, local copies, waits for them, and re-layouts: none -> 5.57 us  [the longest x1 4.32 us: shards(): down_full = jnp.concatenate(list(pieces[5]), axis=1)]
  transfers between devices with their start and end apart: 10 -> 4, of which waited for: 10 -> 3; matrix products, arithmetic and copies ran while one was open for 4% -> 2% of each run, Pallas kernels for 0% -> 61%
where the time goes in v1:
time: 321 us
  Pallas kernels  195 us (61%)
  waiting for transfers between devices  65.1 us (20%)
  matrix products  17.8 us (6%)
  other arithmetic  15 us (5%)
  between operations  13.5 us (4%)
  local copies, waits for them, and re-layouts  8.17 us (3%)
  blocking collectives  5.63 us (2%)
    pallas_call x1, Pallas kernels, gather_all(): pl.pallas_call(functools.partial(gather_kernel, count, len(weights)), out...  195 us
    reduce_scatter x1, waiting for transfers between devices, shards(): lax.psum_scatter(make_rows_product(hidden, down_full).astype(jnp.bfloat16...  26.6 us
    reduce_scatter x1, waiting for transfers between devices, shards(): lax.psum_scatter(make_rows_product(activated, out_full).astype(jnp.bfloat...  24.8 us
    all_gather x1, waiting for transfers between devices, shards(): normed_ffn = lax.all_gather(normed_share, 'tp', axis=0, tiled=True)  13.6 us
  transfers between devices with their start and end apart: 4, of which 3 were waited for; matrix products, arithmetic and copies ran while one was open for 2% of the time, Pallas kernels for 61%

profile of v1, /device:TPU:0, one launch (start us, length us, event | category | flops | bytes accessed | tf_op | source)
XLA Modules:
  0.0 320.5 jit_solution(8497828225935062143)
XLA Ops:
  6.5 0.7 convert_element_type.82
  7.2 1.1 fusion.44
  8.4 1.8 fusion.46
  10.2 0.0 all-gather.3.cloned.1.call-update
  10.3 0.0 reduce-scatter.3.cloned.1.call-start
  10.3 195.1 %shard_map.136 = (bf16[4,512,256]{2,1,0:T(8,128)(2,1)}, bf16[4,512,256]{2,1,0:T(8,128)(2,1)}, bf16[4,256,512]{2,1,0:T(8,128)(2,1)}, bf16[4,512,1280]{2,1,0:T(8,1...) custom-call(bf16[512,256]{1,0:T(8,128)(2,1)} %refs_0_.1, bf16[512,256]{1,0:T(8,128)(2,1)} %refs_1_.1, ...), custom_call_target="tpu_custom_call" | custom-call | tf_op jit(solution)/shard_map/pallas_call | solution.py:192
  205.4 0.0 copy-start.10
  205.4 0.8 dynamic-slice_convert_fusion.3
  206.3 0.7 dynamic-slice_convert_fusion
  207.1 1.3 slice_bitcast_fusion.7
  208.3 0.0 all-gather.3.cloned.1.call-done
  208.4 2.0 fusion.121
  210.4 0.5 fusion.32
  211.0 1.2 fusion.116
  212.2 0.1 reduce_sum.62
  212.3 0.1 reduce_sum.60
  212.3 5.6 %all-reduce.3 = (f32[320]{0:T(512)S(1)}, f32[320]{0:T(512)S(1)}) all-reduce(f32[320]{0:T(512)S(1)} %reduce_sum.62, f32[320]{0:T(512)S(1)} %reduce_sum.60), channel_id=1, replica_groups=mesh['grp'=2,'fs'=4,'tp'=4] {'tp'}, use_global_device_ids=true, to_apply=%region_4.5 | all-reduce | flops 640 | bytes 5120 | tf_op jit(solution)/shard_map/psum | solution.py:257
  218.0 0.2 multiply_convert_fusion
  218.2 0.0 copy-start.4
  218.2 0.0 copy-start.5
  218.2 1.6 convolution_convert_fusion.2
  219.8 0.0 reduce-scatter.3.cloned.1.call-update
  219.8 0.0 all-gather.5.cloned.1.call-start
  219.9 24.8 %reduce-scatter.3.cloned.1.call-done = bf16[80,2048]{1,0:T(8,128)(2,1)} async-done(((bf16[320,2048]{1,0:T(8,128)(2,1)}), bf16[80,2048]{1,0:T(8,128)(2,1)}) %reduce-scatter.3.cloned.1.call-update) | async-done | bytes 327696 | tf_op jit(solution)/shard_map/reduce_scatter | solution.py:269
  244.7 1.1 fusion.40
  245.9 1.3 fusion.48
  247.2 0.9 fusion.50
  248.1 0.0 all-gather.5.cloned.1.call-update
  248.1 0.2 reduce-scatter.5.cloned.1.call-start
  248.4 0.1 dynamic-slice_convert_fusion.2
  248.5 0.1 slice_reduce_fusion.2
  248.5 4.3 %slice_bitcast_fusion.3 = (bf16[1280,512]{1,0:T(8,128)(2,1)S(1)}, bf16[1280,512]{1,0:T(8,128)(2,1)S(1)}, bf16[1280,512]{1,0:T(8,128)(2,1)}, bf16[1280,512]{1,0:T(8,128)(2,1)}) fusion(bf16[4,1280,512]{2,1,0:T(8,128)(2,1)} %get-tuple-element.16), kind=kLoop, calls=%fused_computation.67 | loop fusion | bytes 10485760 | tf_op jit(solution)/shard_map/unstack | solution.py:289
  252.9 13.6 %all-gather.5.cloned.1.call-done = bf16[320,2048]{1,0:T(8,128)(2,1)} async-done(((bf16[80,2048]{1,0:T(8,128)(2,1)}), bf16[320,2048]{1,0:T(8,128)(2,1)}) %all-gather.5.cloned.1.call-update) | async-done | bytes 1310736 | tf_op jit(solution)/shard_map/all_gather | solution.py:279
  266.4 4.7 %convolution_convert_fusion = bf16[320,1280]{1,0:T(8,128)(2,1)S(1)} fusion(bf16[320,2048]{1,0:T(8,128)(2,1)} %all-gather.5.cloned.1.call-done, bf16[2048,1280]{1,0:T(8,128)(2,1)} %bitcast.114), kind=kOutput, calls=%fused_computation.8 | convolution fusion | flops 1678131200 | bytes 7372800 | tf_op jit(solution)/shard_map/dot_general | solution.py:285
  271.2 0.1 convert.5
  271.4 1.2 copy-done.8
  272.5 4.4 %convolution_convert_fusion.1 = bf16[320,1280]{1,0:T(8,128)(2,1)S(1)} fusion(bf16[320,2048]{1,0:T(8,128)(2,1)S(1)} %copy-done.8, bf16[2048,1280]{1,0:T(8,128)(2,1)} %bitcast.113), kind=kOutput, calls=%fused_computation.9 | convolution fusion | flops 1678131200 | bytes 7372800 | tf_op jit(solution)/shard_map/dot_general | solution.py:282
  276.9 0.1 convert.4
  277.0 0.5 fusion.17
  277.5 0.5 fusion.13
  278.0 0.6 fusion.27
  278.6 0.7 copy-done.1
  279.3 0.4 copy-done.2
  279.7 4.6 %fusion.8 = bf16[320,2048]{1,0:T(8,128)(2,1)} fusion(bf16[320,1280]{1,0:T(8,128)(2,1)S(1)} %fusion.27, bf16[1280,512]{1,0:T(8,128)(2,1)S(1)} %get-tuple-element.31, bf16[1280,512]{1,0:T(8,128)(2,1)S(1)} %copy-done.1, bf16[1280,512]{1,0:T(8,128)(2,1)S(1)} %copy-done.2, bf16[1280,512]{1,0:T(8,128)(2,1)S(1)} %get-tuple-element.30), kind=kOutput, calls=%fused_computation.11 | convolution fusion | flops 1699348480 | bytes 7372800 | tf_op jit(solution)/shard_map/dot_general | solution.py:41
  284.4 0.0 reduce-scatter.5.cloned.1.call-update
  284.4 26.6 %reduce-scatter.5.cloned.1.call-done = bf16[80,2048]{1,0:T(8,128)(2,1)} async-done(((bf16[320,2048]{1,0:T(8,128)(2,1)}), bf16[80,2048]{1,0:T(8,128)(2,1)}) %reduce-scatter.5.cloned.1.call-update) | async-done | bytes 327696 | tf_op jit(solution)/shard_map/reduce_scatter | solution.py:290
  311.0 1.1 fusion.42
  312.1 1.9 fusion.51
  (28 shorter events, 0.1 us)
Async XLA Ops:
  6.5 201.8 %all-gather.3.cloned.1.call-start = ((), (), s32[]{:S(2)}) async-start(), calls=%async_computation.2 | async-start | bytes 1638400 | tf_op jit(solution)/shard_map/all_gather | solution.py:245
  10.3 234.5 %reduce-scatter.3.cloned.1.call-start = ((), (), s32[]{:S(2)}) async-start(), calls=%async_computation.3 | async-start | bytes 1638400 | tf_op jit(solution)/shard_map/reduce_scatter | solution.py:269
  205.4 2.9 copy-start.10
  208.4 2.0 copy-start.7
  208.4 2.0 copy-start.9
  218.2 1.7 copy-start.4
  218.2 1.7 copy-start.5
  219.8 26.1 %copy-start = (bf16[80,2048]{1,0:T(8,128)(2,1)S(1)}, bf16[80,2048]{1,0:T(8,128)(2,1)}, u32[]{:S(2)}) copy-start(bf16[80,2048]{1,0:T(8,128)(2,1)} %param.14) | copy-start | bytes 983044
  219.8 28.6 %copy-start.3 = (bf16[2,3,5120]{2,0,1:T(2,128)(2,1)S(1)}, bf16[2,3,5120]{2,0,1:T(2,128)(2,1)}, u32[]{:S(2)}) copy-start(bf16[2,3,5120]{2,0,1:T(2,128)(2,1)} %param.25) | copy-start | bytes 184324
  219.8 46.7 %all-gather.5.cloned.1.call-start = ((), (), s32[]{:S(2)}) async-start(), calls=%async_computation.4 | async-start | bytes 1638400 | tf_op jit(solution)/shard_map/all_gather | solution.py:279
  248.1 62.8 %reduce-scatter.5.cloned.1.call-start = ((), (), s32[]{:S(2)}) async-start(), calls=%async_computation.5 | async-start | bytes 1638400 | tf_op jit(solution)/shard_map/reduce_scatter | solution.py:290
  271.2 1.3 copy-start.8
  278.0 1.3 copy-start.1
  278.0 1.7 copy-start.2
  279.7 4.7 %copy-start.6 = (bf16[2048]{0:T(1024)(128)(2,1)S(1)}, bf16[2048]{0:T(1024)(128)(2,1)}, u32[]{:S(2)}) copy-start(bf16[2048]{0:T(1024)(128)(2,1)} %param.27) | copy-start | bytes 12292
Sparse Core Ops, SparseCore 0:
  10.4 20.8 all-gather.2
  219.9 24.7 reduce-scatter.2
  248.2 18.1 all-gather.4
  284.5 26.4 reduce-scatter.4

commit v2 on v1

--- a/solution.py
+++ b/solution.py
@@ -42,7 +42,8 @@
 
 
 class LineGather:
-    def __init__(self, count, sources, gathered, semaphores):
+    def __init__(self, count, chunks, sources, gathered, semaphores):
+        self.chunks = chunks
         self.count = count
         self.sources = sources
         self.gathered = gathered
@@ -71,15 +72,17 @@
         return self.place >= distance
 
     def rows(self, index, half):
-        size = self.sources[index].shape[0] // 2
-        return pl.ds(pl.multiple_of(half * size, size), size)
+        weight, chunk = divmod(index, self.chunks)
+        half_size = self.sources[weight].shape[0] // 2
+        size = half_size // self.chunks
+        return pl.ds(pl.multiple_of(half * half_size + chunk * size, size), size)
 
     def z_copy(self, index, way, distance):
         step = 1 if way == 0 else -1
         origin = self.place - step * distance
         rows = self.rows(index, self.half)
-        target = self.gathered[index].at[origin, rows]
-        source = self.sources[index].at[rows] if distance == 0 else target
+        target = self.gathered[index // self.chunks].at[origin, rows]
+        source = self.sources[index // self.chunks].at[rows] if distance == 0 else target
         return pltpu.make_async_remote_copy(
             src_ref=source,
             dst_ref=target,
@@ -91,7 +94,7 @@
     def z_arrival(self, index, way, distance):
         step = 1 if way == 0 else -1
         origin = self.place - step * distance
-        target = self.gathered[index].at[origin, self.rows(index, self.half)]
+        target = self.gathered[index // self.chunks].at[origin, self.rows(index, self.half)]
         return pltpu.make_async_remote_copy(
             src_ref=target,
             dst_ref=target,
@@ -104,7 +107,7 @@
         step = 1 if way == 0 else -1
         origin = self.place - step * distance
         half = 1 - self.half if incoming else self.half
-        target = self.gathered[index].at[origin, self.rows(index, half)]
+        target = self.gathered[index // self.chunks].at[origin, self.rows(index, half)]
         return pltpu.make_async_remote_copy(
             src_ref=target,
             dst_ref=target,
@@ -125,7 +128,8 @@
             def _():
                 self.z_copy(index, way, 0).start()
 
-        self.own_copy(index).start()
+        if index % self.chunks == 0:
+            self.own_copy(index // self.chunks).start()
 
     def relay(self, index, distance):
         for way in range(2):
@@ -143,7 +147,8 @@
                 self.y_copy(index, way, distance).start()
 
     def arrive(self, index):
-        self.own_copy(index).wait()
+        if index % self.chunks == 0:
+            self.own_copy(index // self.chunks).wait()
         for distance in range(1, self.count):
             for way in range(2):
 
@@ -168,37 +173,51 @@
                         self.y_copy(index, way, distance).wait_send()
 
 
-def gather_semaphores(weights, count):
-    hops = pltpu.SemaphoreType.DMA((weights, 2, count - 1))
+def gather_semaphores(weights, chunks, count):
+    hops = pltpu.SemaphoreType.DMA((weights * chunks, 2, count - 1))
     return [hops, hops, hops, hops, pltpu.SemaphoreType.DMA((weights,))]
 
 
-def gather_kernel(count, weights, *refs):
-    gather = LineGather(count, refs[:weights], refs[weights : 2 * weights], refs[2 * weights :])
+def gather_kernel(count, weights, chunks, *refs):
+    gather = LineGather(
+        count, chunks, refs[:weights], refs[weights : 2 * weights], refs[2 * weights :]
+    )
+    total = weights * chunks
+    ahead = min(2, total)
     gather.barrier()
-    gather.start(0)
-    for index in range(weights):
-        if index + 1 < weights:
-            gather.start(index + 1)
+    for index in range(ahead):
+        gather.start(index)
+    for index in range(total):
+        if index + ahead < total:
+            gather.start(index + ahead)
         for distance in range(1, count):
             gather.relay(index, distance)
-    for index in range(weights):
+    for index in range(total):
         gather.arrive(index)
-    for index in range(weights):
+    for index in range(total):
         gather.drain(index)
 
 
-def gather_all(count, weights):
-    return pl.pallas_call(
-        functools.partial(gather_kernel, count, len(weights)),
+def gather_all(mesh, weights, call, chunks, after):
+    weights, after = lax.optimization_barrier((tuple(weights), after))
+    if not fits(mesh, weights):
+        return gather_plain(weights), after
+    count = mesh.shape["fs"]
+    held = sum(w.size * w.dtype.itemsize for w in weights)
+    pieces = pl.pallas_call(
+        functools.partial(gather_kernel, count, len(weights), chunks),
         out_shape=[jax.ShapeDtypeStruct((count,) + w.shape, w.dtype) for w in weights],
         in_specs=[pl.BlockSpec(memory_space=pl.ANY)] * len(weights),
         out_specs=[pl.BlockSpec(memory_space=pltpu.VMEM)] * len(weights),
-        scratch_shapes=gather_semaphores(len(weights), count),
+        scratch_shapes=gather_semaphores(len(weights), chunks, count),
+        cost_estimate=pl.CostEstimate(
+            flops=0, bytes_accessed=held * 128, transcendentals=0
+        ),
         compiler_params=pltpu.CompilerParams(
-            collective_id=0, has_side_effects=True, vmem_limit_bytes=60_000_000
+            collective_id=call, has_side_effects=True, vmem_limit_bytes=40_000_000
         ),
     )(*weights)
+    return pieces, after
 
 
 def gather_plain(weights):
@@ -210,7 +229,7 @@
     return (
         mesh.shape["grp"] == 2
         and 2 <= count <= 4
-        and all(w.shape[0] % 64 == 0 and w.shape[1] % 128 == 0 for w in weights)
+        and all(w.shape[0] % 128 == 0 and w.shape[1] % 128 == 0 for w in weights)
         and count * sum(w.size for w in weights) <= 20_000_000
     )
 
@@ -233,15 +252,11 @@
     ffn_post_gain,
 ):
     member = lax.axis_index("tp")
-    weights = (val_weight, gate_weight, out_weight, up_gate_weight, up_val_weight, down_weight)
-    if fits(mesh, weights):
-        pieces = gather_all(mesh.shape["fs"], weights)
-    else:
-        pieces = gather_plain(weights)
-    val_all, gate_all, gate_full, val_full = (
-        pieces[i].reshape(-1, pieces[i].shape[2]) for i in (0, 1, 3, 4)
-    )
     normed_own = rms_scale(tokens.astype(jnp.float32), mix_gain).astype(jnp.bfloat16)
+    mix_pieces, normed_own = gather_all(
+        mesh, (val_weight, gate_weight, out_weight), 0, 2, normed_own
+    )
+    val_all, gate_all = (p.reshape(-1, p.shape[2]) for p in mix_pieces[:2])
     normed = lax.all_gather(normed_own, "tp", axis=0, tiled=True)
     local_ch = val_weight.shape[1]
     values, gate_sums = make_adder(
@@ -265,9 +280,12 @@
     )
     activated = jax.nn.silu((conv_out - chan_mean) * lax.rsqrt(chan_var + chan_epsilon) * own_gain)
     activated = activated.astype(jnp.bfloat16)
-    out_full = jnp.concatenate(list(pieces[2]), axis=1)
+    out_full = jnp.concatenate(list(mix_pieces[2]), axis=1)
+    mix_part = make_rows_product(activated, out_full).astype(jnp.bfloat16)
+    (gate_pieces,), mix_part = gather_all(mesh, (up_gate_weight,), 1, 4, mix_part)
+    gate_full = gate_pieces.reshape(-1, gate_pieces.shape[2])
     mixed_sum = lax.psum_scatter(
-        make_rows_product(activated, out_full).astype(jnp.bfloat16),
+        mix_part,
         "tp",
         scatter_dimension=0,
         tiled=True,
@@ -276,6 +294,8 @@
         jnp.bfloat16
     )
     normed_share = rms_scale(residual.astype(jnp.float32), ffn_gain).astype(jnp.bfloat16)
+    (val_pieces,), normed_share = gather_all(mesh, (up_val_weight,), 2, 4, normed_share)
+    val_full = val_pieces.reshape(-1, val_pieces.shape[2])
     normed_ffn = lax.all_gather(normed_share, "tp", axis=0, tiled=True)
     local_ff = up_gate_weight.shape[1]
     own_ffn_taps = lax.dynamic_slice_in_dim(ffn_taps, member * local_ff, local_ff, 2)
@@ -286,7 +306,8 @@
     gate_conv = depthwise(up_gate, own_ffn_taps[0])
     val_conv = depthwise(up_val, own_ffn_taps[1])
     hidden = (jax.nn.gelu(gate_conv, approximate=True) * val_conv).astype(jnp.bfloat16)
-    down_full = jnp.concatenate(list(pieces[5]), axis=1)
+    (down_pieces,), hidden = gather_all(mesh, (down_weight,), 3, 4, hidden)
+    down_full = jnp.concatenate(list(down_pieces), axis=1)
     ffn_sum = lax.psum_scatter(
         make_rows_product(hidden, down_full).astype(jnp.bfloat16),
         "tp",

time: 321 us -> 323 us (level)
  Pallas kernels: 195 us -> 211 us
  waiting for transfers between devices: 65.1 us -> 50.4 us
    pallas_call x1 -> x4, Pallas kernels: 195 us -> 211 us  [gather_all(): pl.pallas_call(functools.partial(gather_kernel, count, len(weights), chun...]
    all_gather x1, waiting for transfers between devices: 13.6 us -> 0.01 us  [shards(): normed_ffn = lax.all_gather(normed_share, 'tp', axis=0, tiled=True)]
    unnamed x22 -> x56, local copies, waits for them, and re-layouts: 2.33 us -> 9.47 us
    another operation x2, local copies, waits for them, and re-layouts: 5.57 us -> 0.41 us  [the longest x1 0.34 us: shards(): down_full = jnp.concatenate(list(down_pieces), axis=1)]
    reduce_scatter x1, waiting for transfers between devices: 26.6 us -> 23.1 us  [shards(): lax.psum_scatter(make_rows_product(hidden, down_full).astype(jnp.bfloat16...]
  transfers between devices with their start and end apart: 4 -> 4, of which waited for: 3 -> 2; matrix products, arithmetic and copies ran while one was open for 2% -> 1% of each run, Pallas kernels for 61% -> 48%
where the time goes in v2:
time: 323 us; the launch traced here: 322 us
  Pallas kernels  211 us (65%)
  waiting for transfers between devices  50.4 us (16%)
  matrix products  15.5 us (5%)
  other arithmetic  15.4 us (5%)
  between operations  13.7 us (4%)
  local copies, waits for them, and re-layouts  10.7 us (3%)
  blocking collectives  5.63 us (2%)
    pallas_call x4, Pallas kernels, gather_all(): pl.pallas_call(functools.partial(gather_kernel, count, len(weights), chun...  211 us
    reduce_scatter x1, waiting for transfers between devices, shards(): lax.psum_scatter(mix_part, 'tp', scatter_dimension=0, tiled=True)  27.2 us
    reduce_scatter x1, waiting for transfers between devices, shards(): lax.psum_scatter(make_rows_product(hidden, down_full).astype(jnp.bfloat16...  23.1 us
    unnamed x56, local copies, waits for them, and re-layouts  9.47 us
  transfers between devices with their start and end apart: 4, of which 2 were waited for; matrix products, arithmetic and copies ran while one was open for 1% of the time, Pallas kernels for 48%

profile of v2, /device:TPU:0, one launch (start us, length us, event | category | flops | bytes accessed | tf_op | source)
XLA Modules:
  0.0 322.1 jit_solution(1500939928003215889)
XLA Ops:
  6.5 0.7 convert_element_type.82
  7.2 1.1 fusion.44
  8.4 1.8 fusion.46
  10.3 0.0 reduce-scatter.3.cloned.1.call-start
  10.3 0.9 copy-done.6
  11.3 0.9 copy-done.7
  12.2 0.9 copy-done.8
  13.2 39.9 %shard_map.136 = (bf16[4,512,256]{2,1,0:T(8,128)(2,1)S(1)}, bf16[4,512,256]{2,1,0:T(8,128)(2,1)S(1)}, bf16[4,256,512]{2,1,0:T(8,128)(2,1)S(1)}) custom-call(bf16[512,256]{1,0:T(8,128)(2,1)S(1)} %copy-done.6, bf16[512,256]{1,0:T(8,128)(2,1)S(1)} %copy-done.7, bf16[256,512]{1,0:T(8,128)(2,1)S(1)} %copy-done.8), custom_call_target="tpu_custom_call" | custom-call | bytes 100663296 | tf_op jit(solution)/shard_map/pallas_call | solution.py:207
  53.1 1.3 dynamic-slice_convert_fusion.3
  54.4 0.7 dynamic-slice_convert_fusion
  55.1 0.6 fusion.119
  55.8 0.1 slice_bitcast_fusion.7
  55.8 0.0 all-gather.3.cloned.1.call-done
  55.9 1.9 fusion.121
  57.9 0.5 fusion.32
  58.6 1.2 fusion.116
  59.8 0.1 reduce_sum.62
  59.9 0.1 reduce_sum.60
  60.0 5.6 %all-reduce.3 = (f32[320]{0:T(512)S(1)}, f32[320]{0:T(512)S(1)}) all-reduce(f32[320]{0:T(512)S(1)} %reduce_sum.62, f32[320]{0:T(512)S(1)} %reduce_sum.60), channel_id=1, replica_groups=mesh['grp'=2,'fs'=4,'tp'=4] {'tp'}, use_global_device_ids=true, to_apply=%region_4.5 | all-reduce | flops 640 | bytes 5120 | tf_op jit(solution)/shard_map/psum | solution.py:272
  65.6 0.2 multiply_convert_fusion
  65.8 1.6 convolution_convert_fusion.2
  67.5 0.0 all-gather.5.cloned.1.call-start
  67.5 27.2 %reduce-scatter.3.cloned.1.call-done = bf16[80,2048]{1,0:T(8,128)(2,1)} async-done(((bf16[320,2048]{1,0:T(8,128)(2,1)}), bf16[80,2048]{1,0:T(8,128)(2,1)}) %reduce-scatter.3.cloned.1.call-update) | async-done | bytes 327696 | tf_op jit(solution)/shard_map/reduce_scatter | solution.py:287
  94.7 1.1 fusion.40
  95.9 1.3 fusion.48
  97.2 0.9 fusion.50
  98.1 0.0 reduce-scatter.5.cloned.1.call-start
  98.2 0.1 dynamic-slice_convert_fusion.2
  98.3 0.1 slice_reduce_fusion.2
  98.4 60.5 %shard_map.137 = bf16[4,512,1280]{2,1,0:T(8,128)(2,1)S(1)} custom-call(bf16[512,1280]{1,0:T(8,128)(2,1)S(1)} %copy-done.3), custom_call_target="tpu_custom_call" | custom-call | bytes 167772160 | tf_op jit(solution)/shard_map/pallas_call | solution.py:207
  158.9 2.3 copy-done
  161.2 55.4 %shard_map.138 = bf16[4,512,1280]{2,1,0:T(8,128)(2,1)S(1)} custom-call(bf16[512,1280]{1,0:T(8,128)(2,1)S(1)} %copy-done.4), custom_call_target="tpu_custom_call" | custom-call | bytes 167772160 | tf_op jit(solution)/shard_map/pallas_call | solution.py:207
  216.6 2.3 copy-done.2
  218.9 4.9 %convolution_convert_fusion = bf16[320,1280]{1,0:T(8,128)(2,1)S(1)} fusion(bf16[320,2048]{1,0:T(8,128)(2,1)} %all-gather.5.cloned.1.call-done, bf16[2048,1280]{1,0:T(8,128)(2,1)} %bitcast.80), kind=kOutput, calls=%fused_computation.8 | convolution fusion | flops 1678131200 | bytes 7372800 | tf_op jit(solution)/shard_map/dot_general | solution.py:305
  223.8 0.1 convert.5
  224.0 1.2 copy-done.27
  225.1 1.9 convolution_convert_fusion.1
  227.0 0.1 convert.4
  227.2 0.5 fusion.17
  227.7 0.5 fusion.13
  228.2 0.6 fusion.27
  228.7 0.7 copy-done.5
  229.5 54.8 %shard_map.139 = bf16[4,1280,512]{2,1,0:T(8,128)(2,1)S(1)} custom-call(bf16[1280,512]{1,0:T(8,128)(2,1)S(1)} %copy-done.5), custom_call_target="tpu_custom_call" | custom-call | bytes 167772160 | tf_op jit(solution)/shard_map/pallas_call | solution.py:207
  284.3 0.3 slice_bitcast_fusion.3
  284.7 4.7 %fusion.8 = bf16[320,2048]{1,0:T(8,128)(2,1)} fusion(bf16[320,1280]{1,0:T(8,128)(2,1)S(1)} %fusion.27, bf16[1280,512]{1,0:T(8,128)(2,1)S(1)} %get-tuple-element.45, bf16[1280,512]{1,0:T(8,128)(2,1)S(1)} %get-tuple-element.46, bf16[1280,512]{1,0:T(8,128)(2,1)S(1)} %get-tuple-element.47, bf16[1280,512]{1,0:T(8,128)(2,1)S(1)} %get-tuple-element.44), kind=kOutput, calls=%fused_computation.11 | convolution fusion | flops 1699348480 | bytes 7372800 | tf_op jit(solution)/shard_map/dot_general | solution.py:41
  289.4 23.1 %reduce-scatter.5.cloned.1.call-done = bf16[80,2048]{1,0:T(8,128)(2,1)} async-done(((bf16[320,2048]{1,0:T(8,128)(2,1)}), bf16[80,2048]{1,0:T(8,128)(2,1)}) %reduce-scatter.5.cloned.1.call-update) | async-done | bytes 327696 | tf_op jit(solution)/shard_map/reduce_scatter | solution.py:311
  312.5 1.1 fusion.42
  313.7 1.9 fusion.51
  (65 shorter events, 0.3 us)
Async XLA Ops:
  6.5 49.3 %all-gather.3.cloned.1.call-start = ((), (), s32[]{:S(2)}) async-start(), calls=%async_computation.2 | async-start | bytes 1638400 | tf_op jit(solution)/shard_map/all_gather | solution.py:260
  10.3 84.5 %reduce-scatter.3.cloned.1.call-start = ((), (), s32[]{:S(2)}) async-start(), calls=%async_computation.3 | async-start | bytes 1638400 | tf_op jit(solution)/shard_map/reduce_scatter | solution.py:287
  10.3 1.0 copy-start.6
  11.3 0.9 copy-start.7
  12.2 0.9 copy-start.8
  55.9 1.9 copy-start.26
  57.8 0.7 copy-start.11
  57.8 0.7 copy-start.12
  57.8 0.7 copy-start.13
  57.8 0.7 copy-start.14
  57.8 0.7 copy-start.15
  57.9 0.7 copy-start.16
  57.9 0.7 copy-start.17
  57.9 0.7 copy-start.18
  57.9 0.7 copy-start.19
  57.9 0.7 copy-start.20
  57.9 0.7 copy-start.21
  57.9 7.7 %copy-start.22 = (f32[256]{0:T(256)S(1)}, f32[256]{0:T(256)}, u32[]{:S(2)}) copy-start(f32[256]{0:T(256)} %dynamic-slice_convert_fusion.3) | copy-start | bytes 3076
  65.8 1.7 copy-start.23
  65.8 1.7 copy-start.24
  67.4 28.5 %copy-start.9 = (bf16[80,2048]{1,0:T(8,128)(2,1)S(1)}, bf16[80,2048]{1,0:T(8,128)(2,1)}, u32[]{:S(2)}) copy-start(bf16[80,2048]{1,0:T(8,128)(2,1)} %param.14) | copy-start | bytes 983044
  67.4 30.8 %copy-start.10 = (bf16[2,3,5120]{2,0,1:T(2,128)(2,1)S(1)}, bf16[2,3,5120]{2,0,1:T(2,128)(2,1)}, u32[]{:S(2)}) copy-start(bf16[2,3,5120]{2,0,1:T(2,128)(2,1)} %param.25) | copy-start | bytes 184324
  67.4 30.9 %copy-start.3 = (bf16[512,1280]{1,0:T(8,128)(2,1)S(1)}, bf16[512,1280]{1,0:T(8,128)(2,1)}, u32[]{:S(2)}) copy-start(bf16[512,1280]{1,0:T(8,128)(2,1)} %refs_0_.1) | copy-start | bytes 3932164
  67.5 151.5 %all-gather.5.cloned.1.call-start = ((), (), s32[]{:S(2)}) async-start(), calls=%async_computation.4 | async-start | bytes 1638400 | tf_op jit(solution)/shard_map/all_gather | solution.py:299
  98.1 214.4 %reduce-scatter.5.cloned.1.call-start = ((), (), s32[]{:S(2)}) async-start(), calls=%async_computation.5 | async-start | bytes 1638400 | tf_op jit(solution)/shard_map/reduce_scatter | solution.py:311
  98.4 62.8 %copy-start.4 = (bf16[512,1280]{1,0:T(8,128)(2,1)S(1)}, bf16[512,1280]{1,0:T(8,128)(2,1)}, u32[]{:S(2)}) copy-start(bf16[512,1280]{1,0:T(8,128)(2,1)} %refs_0_.2) | copy-start | bytes 3932164
  158.9 2.3 copy-start
  216.6 2.3 copy-start.2
  218.9 5.0 %copy-start.1 = (bf16[4,512,1280]{2,1,0:T(8,128)(2,1)S(1)}, bf16[4,512,1280]{2,1,0:T(8,128)(2,1)}, u32[]{:S(2)}) copy-start(bf16[4,512,1280]{2,1,0:T(8,128)(2,1)} %copy-done) | copy-start | bytes 15728644
  223.8 1.3 copy-start.27
  228.1 1.3 copy-start.5
  284.7 4.7 %copy-start.25 = (bf16[2048]{0:T(1024)(128)(2,1)S(1)}, bf16[2048]{0:T(1024)(128)(2,1)}, u32[]{:S(2)}) copy-start(bf16[2048]{0:T(1024)(128)(2,1)} %param.27) | copy-start | bytes 12292
Sparse Core Ops, SparseCore 0:
  10.4 20.8 all-gather.2
  67.6 27.1 reduce-scatter.2
  98.2 18.1 all-gather.4
  289.5 22.9 reduce-scatter.4

commit v3 on v2

--- a/solution.py
+++ b/solution.py
@@ -282,19 +282,16 @@
     activated = activated.astype(jnp.bfloat16)
     out_full = jnp.concatenate(list(mix_pieces[2]), axis=1)
     mix_part = make_rows_product(activated, out_full).astype(jnp.bfloat16)
-    (gate_pieces,), mix_part = gather_all(mesh, (up_gate_weight,), 1, 4, mix_part)
+    up_weights = (up_gate_weight, up_val_weight)
+    (gate_pieces, val_pieces), mix_part = gather_all(mesh, up_weights, 1, 4, mix_part)
     gate_full = gate_pieces.reshape(-1, gate_pieces.shape[2])
-    mixed_sum = lax.psum_scatter(
-        mix_part,
-        "tp",
-        scatter_dimension=0,
-        tiled=True,
-    ).astype(jnp.float32)
+    mixed_sum = lax.psum_scatter(mix_part, "tp", scatter_dimension=0, tiled=True)
+    mixed_sum = mixed_sum.astype(jnp.float32)
     residual = (tokens.astype(jnp.float32) + rms_scale(mixed_sum, mix_post_gain)).astype(
         jnp.bfloat16
     )
     normed_share = rms_scale(residual.astype(jnp.float32), ffn_gain).astype(jnp.bfloat16)
-    (val_pieces,), normed_share = gather_all(mesh, (up_val_weight,), 2, 4, normed_share)
+    (down_pieces,), normed_share = gather_all(mesh, (down_weight,), 2, 4, normed_share)
     val_full = val_pieces.reshape(-1, val_pieces.shape[2])
     normed_ffn = lax.all_gather(normed_share, "tp", axis=0, tiled=True)
     local_ff = up_gate_weight.shape[1]
@@ -306,7 +303,6 @@
     gate_conv = depthwise(up_gate, own_ffn_taps[0])
     val_conv = depthwise(up_val, own_ffn_taps[1])
     hidden = (jax.nn.gelu(gate_conv, approximate=True) * val_conv).astype(jnp.bfloat16)
-    (down_pieces,), hidden = gather_all(mesh, (down_weight,), 3, 4, hidden)
     down_full = jnp.concatenate(list(down_pieces), axis=1)
     ffn_sum = lax.psum_scatter(
         make_rows_product(hidden, down_full).astype(jnp.bfloat16),

time: 323 us -> 312 us (0.966)
  Pallas kernels: 211 us -> 199 us
    pallas_call x4 -> x3, Pallas kernels: 211 us -> 199 us  [gather_all(): pl.pallas_call(functools.partial(gather_kernel, count, len(weights), chun...]
    unnamed x56 -> x60, local copies, waits for them, and re-layouts: 9.47 us -> 7.56 us
  transfers between devices with their start and end apart: 4 -> 4, of which waited for: 2 -> 2; matrix products, arithmetic and copies ran while one was open for 1% -> 2% of each run, Pallas kernels for 48% -> 64%
where the time goes in v3:
time: 312 us; the launch traced here: 311 us
  Pallas kernels  199 us (64%)
  waiting for transfers between devices  51.6 us (17%)
  other arithmetic  15.4 us (5%)
  matrix products  15.4 us (5%)
  between operations  13.7 us (4%)
  local copies, waits for them, and re-layouts  10.6 us (3%)
  blocking collectives  5.63 us (2%)
    pallas_call x3, Pallas kernels, gather_all(): pl.pallas_call(functools.partial(gather_kernel, count, len(weights), chun...  199 us
    reduce_scatter x1, waiting for transfers between devices, shards(): lax.psum_scatter(mix_part, 'tp', scatter_dimension=0, tiled=True)  27.2 us
    reduce_scatter x1, waiting for transfers between devices, shards(): lax.psum_scatter(make_rows_product(hidden, down_full).astype(jnp.bfloat16...  24.3 us
    unnamed x60, local copies, waits for them, and re-layouts  7.56 us
  transfers between devices with their start and end apart: 4, of which 2 were waited for; matrix products, arithmetic and copies ran while one was open for 2% of the time, Pallas kernels for 64%

profile of v3, /device:TPU:0, one launch (start us, length us, event | category | flops | bytes accessed | tf_op | source)
XLA Modules:
  0.0 311.3 jit_solution(11465710684752397244)
XLA Ops:
  6.5 0.7 convert_element_type.82
  7.2 1.1 fusion.44
  8.4 1.8 fusion.46
  10.3 0.0 reduce-scatter.3.cloned.1.call-start
  10.3 0.9 copy-done.3
  11.3 0.9 copy-done.4
  12.2 0.9 copy-done.5
  13.2 39.9 %shard_map.136 = (bf16[4,512,256]{2,1,0:T(8,128)(2,1)S(1)}, bf16[4,512,256]{2,1,0:T(8,128)(2,1)S(1)}, bf16[4,256,512]{2,1,0:T(8,128)(2,1)S(1)}) custom-call(bf16[512,256]{1,0:T(8,128)(2,1)S(1)} %copy-done.3, bf16[512,256]{1,0:T(8,128)(2,1)S(1)} %copy-done.4, bf16[256,512]{1,0:T(8,128)(2,1)S(1)} %copy-done.5), custom_call_target="tpu_custom_call" | custom-call | bytes 100663296 | tf_op jit(solution)/shard_map/pallas_call | solution.py:207
  53.1 1.3 dynamic-slice_convert_fusion.3
  54.4 0.7 dynamic-slice_convert_fusion
  55.1 0.6 fusion.119
  55.8 0.1 slice_bitcast_fusion.7
  55.8 0.0 all-gather.3.cloned.1.call-done
  55.9 1.9 fusion.121
  57.9 0.5 fusion.32
  58.6 1.2 fusion.116
  59.8 0.1 reduce_sum.60
  59.9 0.1 reduce_sum.62
  60.0 5.6 %all-reduce.3 = (f32[320]{0:T(512)S(1)}, f32[320]{0:T(512)S(1)}) all-reduce(f32[320]{0:T(512)S(1)} %reduce_sum.62, f32[320]{0:T(512)S(1)} %reduce_sum.60), channel_id=1, replica_groups=mesh['grp'=2,'fs'=4,'tp'=4] {'tp'}, use_global_device_ids=true, to_apply=%region_4.5 | all-reduce | flops 640 | bytes 5120 | tf_op jit(solution)/shard_map/psum | solution.py:272
  65.6 0.2 multiply_convert_fusion
  65.8 1.6 convolution_convert_fusion.2
  67.5 0.0 reduce-scatter.3.cloned.1.call-update
  67.5 0.0 all-gather.5.cloned.1.call-start
  67.6 27.2 %reduce-scatter.3.cloned.1.call-done = bf16[80,2048]{1,0:T(8,128)(2,1)} async-done(((bf16[320,2048]{1,0:T(8,128)(2,1)}), bf16[80,2048]{1,0:T(8,128)(2,1)}) %reduce-scatter.3.cloned.1.call-update) | async-done | bytes 327696 | tf_op jit(solution)/shard_map/reduce_scatter | solution.py:288
  94.8 1.1 fusion.40
  95.9 1.3 fusion.48
  97.2 0.9 fusion.50
  98.1 0.0 reduce-scatter.5.cloned.1.call-start
  98.2 0.1 dynamic-slice_convert_fusion.2
  98.3 0.1 slice_reduce_fusion.2
  98.4 103.5 %shard_map.137 = (bf16[4,512,1280]{2,1,0:T(8,128)(2,1)S(1)}, bf16[4,512,1280]{2,1,0:T(8,128)(2,1)S(1)}) custom-call(bf16[512,1280]{1,0:T(8,128)(2,1)S(1)} %copy-done, bf16[512,1280]{1,0:T(8,128)(2,1)S(1)} %copy-done.1), custom_call_target="tpu_custom_call" | custom-call | bytes 335544320 | tf_op jit(solution)/shard_map/pallas_call | solution.py:207
  202.0 2.3 copy-done.8
  204.3 55.4 %shard_map.138 = bf16[4,1280,512]{2,1,0:T(8,128)(2,1)S(1)} custom-call(bf16[1280,512]{1,0:T(8,128)(2,1)S(1)} %copy-done.2), custom_call_target="tpu_custom_call" | custom-call | bytes 167772160 | tf_op jit(solution)/shard_map/pallas_call | solution.py:207
  259.7 2.0 slice_bitcast_fusion.3
  261.8 4.9 %convolution_convert_fusion.1 = bf16[320,1280]{1,0:T(8,128)(2,1)S(1)} fusion(bf16[320,2048]{1,0:T(8,128)(2,1)} %all-gather.5.cloned.1.call-done, bf16[2048,1280]{1,0:T(8,128)(2,1)} %bitcast.80), kind=kOutput, calls=%fused_computation.9 | convolution fusion | flops 1678131200 | bytes 7372800 | tf_op jit(solution)/shard_map/dot_general | solution.py:299
  266.7 0.1 convert.4
  266.8 1.2 copy-done.29
  268.0 1.9 convolution_convert_fusion
  269.9 0.1 convert.5
  270.0 0.5 fusion.13
  270.5 0.5 fusion.17
  271.0 0.6 fusion.27
  271.6 0.7 copy-done.10
  272.3 0.4 copy-done.11
  272.7 4.6 %fusion.8 = bf16[320,2048]{1,0:T(8,128)(2,1)} fusion(bf16[320,1280]{1,0:T(8,128)(2,1)S(1)} %fusion.27, bf16[1280,512]{1,0:T(8,128)(2,1)S(1)} %get-tuple-element.47, bf16[1280,512]{1,0:T(8,128)(2,1)S(1)} %copy-done.10, bf16[1280,512]{1,0:T(8,128)(2,1)S(1)} %copy-done.11, bf16[1280,512]{1,0:T(8,128)(2,1)S(1)} %get-tuple-element.46), kind=kOutput, calls=%fused_computation.11 | convolution fusion | flops 1699348480 | bytes 7372800 | tf_op jit(solution)/shard_map/dot_general | solution.py:41
  277.4 24.3 %reduce-scatter.5.cloned.1.call-done = bf16[80,2048]{1,0:T(8,128)(2,1)} async-done(((bf16[320,2048]{1,0:T(8,128)(2,1)}), bf16[80,2048]{1,0:T(8,128)(2,1)}) %reduce-scatter.5.cloned.1.call-update) | async-done | bytes 327696 | tf_op jit(solution)/shard_map/reduce_scatter | solution.py:307
  301.7 1.1 fusion.42
  302.8 1.9 fusion.51
  (68 shorter events, 0.2 us)
Async XLA Ops:
  6.5 49.3 %all-gather.3.cloned.1.call-start = ((), (), s32[]{:S(2)}) async-start(), calls=%async_computation.2 | async-start | bytes 1638400 | tf_op jit(solution)/shard_map/all_gather | solution.py:260
  10.3 84.5 %reduce-scatter.3.cloned.1.call-start = ((), (), s32[]{:S(2)}) async-start(), calls=%async_computation.3 | async-start | bytes 1638400 | tf_op jit(solution)/shard_map/reduce_scatter | solution.py:288
  10.3 1.0 copy-start.3
  11.3 0.9 copy-start.4
  12.2 0.9 copy-start.5
  55.9 1.9 copy-start.28
  57.8 0.7 copy-start.13
  57.8 0.7 copy-start.14
  57.8 0.7 copy-start.15
  57.9 0.7 copy-start.16
  57.9 0.7 copy-start.17
  57.9 0.7 copy-start.18
  57.9 0.7 copy-start.19
  57.9 0.7 copy-start.20
  57.9 0.7 copy-start.21
  57.9 0.7 copy-start.22
  57.9 0.7 copy-start.23
  57.9 7.7 %copy-start.24 = (f32[256]{0:T(256)S(1)}, f32[256]{0:T(256)}, u32[]{:S(2)}) copy-start(f32[256]{0:T(256)} %dynamic-slice_convert_fusion.3) | copy-start | bytes 3076
  65.8 1.7 copy-start.25
  65.8 1.7 copy-start.26
  67.4 28.5 %copy-start.9 = (bf16[80,2048]{1,0:T(8,128)(2,1)S(1)}, bf16[80,2048]{1,0:T(8,128)(2,1)}, u32[]{:S(2)}) copy-start(bf16[80,2048]{1,0:T(8,128)(2,1)} %param.14) | copy-start | bytes 983044
  67.4 30.8 %copy-start.12 = (bf16[2,3,5120]{2,0,1:T(2,128)(2,1)S(1)}, bf16[2,3,5120]{2,0,1:T(2,128)(2,1)}, u32[]{:S(2)}) copy-start(bf16[2,3,5120]{2,0,1:T(2,128)(2,1)} %param.25) | copy-start | bytes 184324
  67.4 31.0 %copy-start = (bf16[512,1280]{1,0:T(8,128)(2,1)S(1)}, bf16[512,1280]{1,0:T(8,128)(2,1)}, u32[]{:S(2)}) copy-start(bf16[512,1280]{1,0:T(8,128)(2,1)} %refs_0_.1) | copy-start | bytes 3932164
  67.4 31.0 %copy-start.1 = (bf16[512,1280]{1,0:T(8,128)(2,1)S(1)}, bf16[512,1280]{1,0:T(8,128)(2,1)}, u32[]{:S(2)}) copy-start(bf16[512,1280]{1,0:T(8,128)(2,1)} %refs_1_.1) | copy-start | bytes 3932164
  67.5 194.3 %all-gather.5.cloned.1.call-start = ((), (), s32[]{:S(2)}) async-start(), calls=%async_computation.4 | async-start | bytes 1638400 | tf_op jit(solution)/shard_map/all_gather | solution.py:296
  98.1 203.5 %reduce-scatter.5.cloned.1.call-start = ((), (), s32[]{:S(2)}) async-start(), calls=%async_computation.5 | async-start | bytes 1638400 | tf_op jit(solution)/shard_map/reduce_scatter | solution.py:307
  98.2 106.1 %copy-start.2 = (bf16[1280,512]{1,0:T(8,128)(2,1)S(1)}, bf16[1280,512]{1,0:T(8,128)(2,1)}, u32[]{:S(2)}) copy-start(bf16[1280,512]{1,0:T(8,128)(2,1)} %refs_0_.2) | copy-start | bytes 3932164
  202.0 2.3 copy-start.8
  204.3 55.4 %copy-start.6 = (bf16[4,512,1280]{2,1,0:T(8,128)(2,1)}, bf16[4,512,1280]{2,1,0:T(8,128)(2,1)S(1)}, u32[]{:S(2)}) copy-start(bf16[4,512,1280]{2,1,0:T(8,128)(2,1)S(1)} %get-tuple-element.31) | copy-start | bytes 15728644
  261.8 5.0 %copy-start.7 = (bf16[4,512,1280]{2,1,0:T(8,128)(2,1)S(1)}, bf16[4,512,1280]{2,1,0:T(8,128)(2,1)}, u32[]{:S(2)}) copy-start(bf16[4,512,1280]{2,1,0:T(8,128)(2,1)} %copy-done.6) | copy-start | bytes 15728644
  266.7 1.3 copy-start.29
  271.0 1.3 copy-start.10
  271.0 1.7 copy-start.11
  272.7 4.7 %copy-start.27 = (bf16[2048]{0:T(1024)(128)(2,1)S(1)}, bf16[2048]{0:T(1024)(128)(2,1)}, u32[]{:S(2)}) copy-start(bf16[2048]{0:T(1024)(128)(2,1)} %param.27) | copy-start | bytes 12292
Sparse Core Ops, SparseCore 0:
  10.4 20.8 all-gather.2
  67.6 27.1 reduce-scatter.2
  98.3 18.1 all-gather.4
  277.5 24.1 reduce-scatter.4
